TPU v7x, 32 devices: a whole 2x2x4 slice. The times are simulated.
32 devices in a mesh: sp: 8 (over z, x), tp: 4 (over y, core).
Axes of the slice: x: 2, y: 2, z: 4, core: 2. Of those that a mesh axis runs over, the one named last changes fastest.
Arguments:
- queries: bfloat16 [4096, 2048], P('sp', 'tp'), may hold values from -90 to 90, as said below
- key_rows: bfloat16 [4096, 512], P('sp', 'tp'), may hold values from -6 to 6
- value_rows: bfloat16 [4096, 512], P('sp', 'tp'), may hold values from -6 to 6
- sink_logits: float32 [16], P('tp'), may hold values from 2 to 7
- residual: bfloat16 [4096, 2048], P('sp'), may hold values from -6 to 6
- norm_gain: float32 [2048], replicated, may hold values from 0.1 to 1.9
- out_weight: bfloat16 [2048, 2048], P('tp'), may hold values from -1.5 to 1.5
- gate_weight: bfloat16 [2048, 5632], P('sp', 'tp'), may hold values from -0.125 to 0.125
- up_weight: bfloat16 [2048, 5632], P('sp', 'tp'), may hold values from -0.125 to 0.125
- down_weight: bfloat16 [5632, 2048], P('tp', 'sp'), may hold values from -0.078125 to 0.078125
Outputs:
- mixed: bfloat16 [4096, 2048], P(('sp', 'tp'))
Inputs may be any that keep to these rules, and one draw needn't show every extreme that they name: queries are mostly of order one; some rows may be much larger.
All inputs are finite; a program needn't handle non-finite values.
Results may differ from a plain program's by a relative error of at most 0.012.
Values may be sent and summed in bfloat16 or wider, within the bound.
A program may use at most 128 MiB of HBM per device.

v0:
```python
import jax
import jax.numpy as jnp
from jax import lax
from jax.sharding import PartitionSpec as P

DH = 128
WIN = 128
EPSILON = 1e-06
MASKED = -1e30


def with_halo(cells, sides, width):
    for axis, dim in sides:
        count = lax.axis_size(axis)
        ends = count - 1
        head = lax.slice_in_dim(cells, 0, width, axis=dim)
        tail = lax.slice_in_dim(cells, cells.shape[dim] - width, cells.shape[dim], axis=dim)
        cells = jnp.concatenate(
            [
                lax.ppermute(tail, axis, [(i, (i + 1) % count) for i in range(ends)]),
                cells,
                lax.ppermute(head, axis, [((i + 1) % count, i) for i in range(ends)]),
            ],
            axis=dim,
        )
    return cells


def attend_block(query_blk, key_blk, value_blk, sink_logits, query_pos, key_pos, seq_len):
    kv_heads = key_blk.shape[1] // DH
    group_size = query_blk.shape[1] // key_blk.shape[1]
    query_four = query_blk.reshape(query_blk.shape[0], kv_heads, group_size, DH)
    key_three = key_blk.reshape(key_blk.shape[0], kv_heads, DH)
    value_three = value_blk.reshape(value_blk.shape[0], kv_heads, DH)
    scores = jnp.einsum(
        "qhgd,khd->hgqk", query_four, key_three, preferred_element_type=jnp.float32
    ) * DH ** (-0.5)
    allowed = (
        (jnp.abs(key_pos[None, :] - query_pos[:, None]) <= WIN)
        & (key_pos[None, :] >= 0)
        & (key_pos[None, :] < seq_len)
    )
    scores = jnp.where(allowed[None, None], scores, MASKED)
    sink_col = sink_logits.reshape(kv_heads, group_size)[:, :, None]
    highest = jnp.maximum(jnp.max(scores, axis=-1), sink_col)
    weights_exp = jnp.exp(scores - highest[..., None])
    denominator = jnp.sum(weights_exp, axis=-1) + jnp.exp(sink_col - highest)
    probabilities = (weights_exp / denominator[..., None]).astype(jnp.bfloat16)
    heads_out = jnp.einsum(
        "hgqk,khd->qhgd", probabilities, value_three, preferred_element_type=jnp.float32
    )
    return heads_out.astype(jnp.bfloat16).reshape(query_blk.shape[0], kv_heads * group_size * DH)


def rms_scale(rows_wide, norm_gain):
    mean_square = jnp.mean(rows_wide * rows_wide, axis=-1, keepdims=True)
    return (rows_wide * lax.rsqrt(mean_square + EPSILON) * norm_gain).astype(jnp.bfloat16)


def fetch_down(down_weight):
    return lax.all_gather(down_weight, "sp", axis=1, tiled=True)


def shards(
    queries,
    key_rows,
    value_rows,
    sink_logits,
    residual,
    norm_gain,
    out_weight,
    gate_weight,
    up_weight,
    down_weight,
):
    tok_local = queries.shape[0]
    block_len = 2 * WIN
    share_rows = tok_local // lax.axis_size("tp")
    seq_len = tok_local * lax.axis_size("sp")
    device_offset = lax.axis_index("sp") * tok_local
    kv_pair = jnp.stack([key_rows, value_rows])
    kv_ext = with_halo(kv_pair, (("sp", 1),), WIN)

    def one_block(block_index):
        block_first = block_index * block_len
        query_blk = lax.dynamic_slice_in_dim(queries, block_first, block_len, 0)
        key_blk = lax.dynamic_slice_in_dim(kv_ext[0], block_first, block_len + 2 * WIN, 0)
        value_blk = lax.dynamic_slice_in_dim(kv_ext[1], block_first, block_len + 2 * WIN, 0)
        query_pos = device_offset + block_first + jnp.arange(block_len, dtype=jnp.int32)
        key_pos = (
            device_offset + block_first - WIN + jnp.arange(block_len + 2 * WIN, dtype=jnp.int32)
        )
        return attend_block(query_blk, key_blk, value_blk, sink_logits, query_pos, key_pos, seq_len)

    blocks = lax.map(one_block, jnp.arange(tok_local // block_len, dtype=jnp.int32))
    attended = blocks.reshape(tok_local, queries.shape[1])
    own_first = lax.axis_index("tp") * share_rows
    attn_full = lax.psum(
        jnp.dot(attended, out_weight, preferred_element_type=jnp.float32).astype(jnp.bfloat16), "tp"
    ).astype(jnp.float32)
    middle_all = residual.astype(jnp.float32) + attn_full
    normed_all = rms_scale(middle_all, norm_gain)
    middle_own = lax.dynamic_slice_in_dim(middle_all, own_first, share_rows, 0)
    gate_sectioned = lax.all_gather(gate_weight, "sp", axis=0, tiled=True)
    up_sectioned = lax.all_gather(up_weight, "sp", axis=0, tiled=True)
    gate_acc = jnp.dot(normed_all, gate_sectioned, preferred_element_type=jnp.float32)
    up_acc = jnp.dot(normed_all, up_sectioned, preferred_element_type=jnp.float32)
    down_whole = fetch_down(down_weight)
    hidden = (jax.nn.silu(gate_acc) * up_acc).astype(jnp.bfloat16)
    ffn_share = lax.psum_scatter(
        jnp.dot(hidden, down_whole, preferred_element_type=jnp.float32).astype(jnp.bfloat16),
        "tp",
        scatter_dimension=0,
        tiled=True,
    ).astype(jnp.float32)
    return (middle_own + ffn_share).astype(jnp.bfloat16)


def solution(mesh):
    placed = (
        P("sp", "tp"),
        P("sp", "tp"),
        P("sp", "tp"),
        P("tp"),
        P("sp", None),
        P(),
        P("tp", None),
        P("sp", "tp"),
        P("sp", "tp"),
        P("tp", "sp"),
    )
    return jax.shard_map(
        shards, mesh=mesh, in_specs=placed, out_specs=P(("sp", "tp"), None), check_vma=False
    )
```

profile of v0, /device:TPU:0, one launch (start us, length us, event | category | flops | bytes accessed | tf_op | source)
XLA Modules:
  0.0 370.6 jit_solution(8707252518556242722)
XLA Ops:
  7.4 1.0 pad_maximum_fusion.2
  8.3 4.9 %collective-permute-start = (bf16[2,128,128]{2,1,0:T(8,128)(2,1)S(1)}, bf16[2,128,128]{2,1,0:T(8,128)(2,1)S(1)}, u32[]{:S(2)}, u32[]{:S(2)}) collective-permute-start(bf16[2,128,128]{2,1,0:T(8,128)(2,1)S(1)} %get-tuple-element.124), channel_id=1, source_target_pairs={{0,4},{4,8},{8,12},{12,16},{16,20},{20,24},{24,28},{1,5},{5,9},{9,... | collective-permute-start | bytes 196616 | tf_op jit(solution)/shard_map/ppermute | solution.py:20
  13.2 1.3 collective-permute-start.1
  14.5 0.6 collective-permute-done
  15.1 4.3 %collective-permute-done.1 = bf16[2,128,128]{2,1,0:T(8,128)(2,1)S(1)} collective-permute-done((bf16[2,128,128]{2,1,0:T(8,128)(2,1)S(1)}, bf16[2,128,128]{2,1,0:T(8,128)(2,1)S(1)}, u32[]{:S(2)}, u32[]{:S(2)}) %collective-permute-start.1) | collective-permute-done | bytes 65568 | tf_op jit(solution)/shard_map/ppermute | solution.py:22
  19.4 1.0 pad_maximum_fusion
  20.4 11.1 %while.12 = (s32[]{:T(128)}, bf16[2,256,512]{2,1,0:T(8,128)(2,1)}, bf16[2,768,128]{2,1,0:T(8,128)(2,1)S(1)}, s32[2]{0:T(128)S(1)}, s32[]{:T(128)}, /*index=5*/bf...) while((s32[]{:T(128)}, bf16[2,256,512]{2,1,0:T(8,128)(2,1)}, ...), condition=%wide.region_3.4_spmd, body=%wide.region_0.3_spmd.sunk | while | flops 273420544 | bytes 14467512 | solution.py:95
  20.4 0.6 dynamic_slice.42
  21.7 0.3 fusion.36
  22.0 1.0 constant_dynamic-slice_fusion.2
  23.0 0.1 copy.25
  23.2 0.5 fusion.37
  23.7 0.1 broadcast_maximum_fusion.2
  23.7 0.3 fusion.38
  24.0 0.1 exponential_add_fusion.2
  24.1 0.5 convolution_convert_fusion.4
  24.6 0.1 copy.26
  24.8 0.4 copy-done.2
  25.2 0.8 copy-done.3
  26.0 0.6 dynamic_slice.42
  27.3 0.3 fusion.36
  27.6 1.0 constant_dynamic-slice_fusion.2
  28.5 0.1 copy.25
  28.7 0.5 fusion.37
  29.2 0.1 broadcast_maximum_fusion.2
  29.3 0.3 fusion.38
  29.6 0.1 exponential_add_fusion.2
  29.7 0.5 convolution_convert_fusion.4
  30.2 0.1 copy.26
  30.3 0.4 copy-done.2
  30.7 0.8 copy-done.3
  31.5 3.6 convolution_convert_fusion.1
  35.2 0.0 all-gather.4.cloned.1.call-start
  35.3 0.5 all-gather.4.cloned.1.call-update
  35.8 0.0 all-gather.6.cloned.1.call-start
  35.8 0.5 all-gather.6.cloned.1.call-update
  36.4 0.0 all-gather.8.cloned.1.call-start
  36.4 0.5 all-gather.8.cloned.1.call-update
  37.0 0.0 reduce-scatter.2.cloned.1.call-start
  37.0 50.9 %all-reduce.2.cloned.1.call-done = bf16[512,2048]{1,0:T(8,128)(2,1)} async-done(((bf16[512,2048]{1,0:T(8,128)(2,1)}), bf16[512,2048]{1,0:T(8,128)(2,1)}) %all-reduce.2.cloned.1.call-update) | async-done | bytes 2097168 | tf_op jit(solution)/shard_map/psum | solution.py:98
  87.9 4.9 %convert_add_fusion = (f32[512,2048]{1,0:T(8,128)}, f32[512]{0:T(512)S(1)}) fusion(bf16[512,2048]{1,0:T(8,128)(2,1)} %all-reduce.2.cloned.1.call-done, bf16[512,2048]{1,0:T(8,128)(2,1)} %param.16), kind=kLoop, calls=%fused_computation.25 | loop fusion | flops 5242368 | bytes 8390656 | tf_op jit(solution)/shard_map/add | solution.py:101
  92.8 38.4 %all-gather.4.cloned.1.call-done = bf16[2048,1408]{1,0:T(8,128)(2,1)} async-done(((bf16[256,1408]{1,0:T(8,128)(2,1)}), bf16[2048,1408]{1,0:T(8,128)(2,1)}) %all-gather.4.cloned.1.call-update) | async-done | bytes 5767184 | tf_op jit(solution)/shard_map/all_gather | solution.py:104
  131.2 9.0 %fusion.14 = f32[512,1408]{1,0:T(8,128)} fusion(bf16[2048,1408]{1,0:T(8,128)(2,1)} %all-gather.4.cloned.1.call-done, f32[2048]{0:T(1024)S(1)} %copy-done.4, f32[512]{0:T(512)S(1)} %add_rsqrt_fusion, bf16[512,2048]{1,0:T(8,128)(2,1)} %all-reduce.2.cloned.1.call-done, bf16[512,2048]{1,0:T(8,128)(2,1)} %param.16), kind=kOutput, calls=%fused_computation.36 | convolution fusion | flops 2959081472 | bytes 12855296 | tf_op jit(solution)/shard_map/dot_general | solution.py:106
  140.2 83.4 %all-gather.6.cloned.1.call-done = bf16[2048,1408]{1,0:T(8,128)(2,1)} async-done(((bf16[256,1408]{1,0:T(8,128)(2,1)}), bf16[2048,1408]{1,0:T(8,128)(2,1)}) %all-gather.6.cloned.1.call-update) | async-done | bytes 5767184 | tf_op jit(solution)/shard_map/all_gather | solution.py:105
  223.6 93.0 %all-gather.8.cloned.1.call-done = bf16[1408,2048]{1,0:T(8,128)(2,1)} async-done(((bf16[1408,256]{1,0:T(8,128)(2,1)}), bf16[1408,2048]{1,0:T(8,128)(2,1)}) %all-gather.8.cloned.1.call-update) | async-done | bytes 5767184 | tf_op jit(solution)/shard_map/all_gather | solution.py:61
  316.5 14.6 %convolution_convert_fusion.2 = bf16[512,2048]{1,0:T(8,128)(2,1)} fusion(bf16[1408,2048]{1,0:T(8,128)(2,1)} %all-gather.8.cloned.1.call-done, bf16[2048,1408]{1,0:T(8,128)(2,1)} %all-gather.6.cloned.1.call-done, f32[512,1408]{1,0:T(8,128)} %fusion.14, f32[2048]{0:T(1024)S(1)} %copy-done.4, f32[512]{0:T(512)S(1)} %add_rsqrt_fusion, ...), kind=kOutput, calls=%fused_computation.29 | convolution fusion | flops 5917245440 | bytes 20719616 | tf_op jit(solution)/shard_map/dot_general | solution.py:111
  331.2 29.5 %reduce-scatter.2.cloned.1.call-done = bf16[128,2048]{1,0:T(8,128)(2,1)} async-done(((bf16[512,2048]{1,0:T(8,128)(2,1)}), bf16[128,2048]{1,0:T(8,128)(2,1)}) %reduce-scatter.2.cloned.1.call-update) | async-done | bytes 524304 | tf_op jit(solution)/shard_map/reduce_scatter | solution.py:110
  360.7 2.3 add_convert_fusion
  (28 shorter events, 0.2 us)
Async XLA Ops:
  7.4 24.2 %copy-start = (bf16[512,2048]{1,0:T(8,128)(2,1)S(1)}, bf16[512,2048]{1,0:T(8,128)(2,1)}, u32[]{:S(2)}) copy-start(bf16[512,2048]{1,0:T(8,128)(2,1)} %param.18) | copy-start | bytes 6291460
  7.4 80.6 %all-reduce.2.cloned.1.call-start = ((), (), s32[]{:S(2)}) async-start(), calls=%async_computation.1 | async-start | bytes 4194304 | tf_op jit(solution)/shard_map/psum | solution.py:98
  8.3 6.8 %collective-permute-start = (bf16[2,128,128]{2,1,0:T(8,128)(2,1)S(1)}, bf16[2,128,128]{2,1,0:T(8,128)(2,1)S(1)}, u32[]{:S(2)}, u32[]{:S(2)}) collective-permute-start(bf16[2,128,128]{2,1,0:T(8,128)(2,1)S(1)} %get-tuple-element.124), channel_id=1, source_target_pairs={{0,4},{4,8},{8,12},{12,16},{16,20},{20,24},{24,28},{1,5},{5,9},{9,... | collective-permute-start | bytes 196616 | tf_op jit(solution)/shard_map/ppermute | solution.py:20
  13.2 6.2 %collective-permute-start.1 = (bf16[2,128,128]{2,1,0:T(8,128)(2,1)S(1)}, bf16[2,128,128]{2,1,0:T(8,128)(2,1)S(1)}, u32[]{:S(2)}, u32[]{:S(2)}) collective-permute-start(bf16[2,128,128]{2,1,0:T(8,128)(2,1)S(1)} %get-tuple-element.125), channel_id=1, source_target_pairs={{4,0},{8,4},{12,8},{16,12},{20,16},{24,20},{28,24},{5,1},{9,5},{13... | collective-permute-start | bytes 196616 | tf_op jit(solution)/shard_map/ppermute | solution.py:22
  20.4 3.2 copy-start.1
  24.1 1.0 copy-start.2
  25.2 0.8 copy-start.3
  26.0 3.2 copy-start.1
  29.7 1.0 copy-start.2
  30.7 0.8 copy-start.3
  35.2 96.0 %all-gather.4.cloned.1.call-start = ((), (), s32[]{:S(2)}) async-start(), calls=%async_computation.2 | async-start | bytes 6488064 | tf_op jit(solution)/shard_map/all_gather | solution.py:104
  35.8 187.8 %all-gather.6.cloned.1.call-start = ((), (), s32[]{:S(2)}) async-start(), calls=%async_computation.3 | async-start | bytes 6488064 | tf_op jit(solution)/shard_map/all_gather | solution.py:105
  36.4 280.2 %all-gather.8.cloned.1.call-start = ((), (), s32[]{:S(2)}) async-start(), calls=%async_computation.4 | async-start | bytes 6488064 | tf_op jit(solution)/shard_map/all_gather | solution.py:61
  37.0 94.3 %copy-start.4 = (f32[2048]{0:T(1024)S(1)}, f32[2048]{0:T(1024)}, u32[]{:S(2)}) copy-start(f32[2048]{0:T(1024)} %param.17) | copy-start | bytes 24580
  37.0 323.7 %reduce-scatter.2.cloned.1.call-start = ((), (), s32[]{:S(2)}) async-start(), calls=%async_computation.5 | async-start | bytes 2621440 | tf_op jit(solution)/shard_map/reduce_scatter | solution.py:110
Sparse Core Ops, SparseCore 0:
  35.3 52.5 all-reduce.1
  331.3 29.3 reduce-scatter.1
Sparse Core Ops, SparseCore 1:
  37.9 93.3 all-gather.3
  133.3 90.2 all-gather.5
  225.5 91.0 all-gather.7
where the time goes:
time: 371 us
  waiting for transfers between devices  302 us (81%)
  matrix products  29.2 us (8%)
  between operations  15.1 us (4%)
  other arithmetic  10.6 us (3%)
  starting transfers between devices  6.34 us (2%)
  local copies, waits for them, and re-layouts  6.13 us (2%)
    all_gather x1, waiting for transfers between devices, fetch_down(): return lax.all_gather(down_weight, 'sp', axis=1, tiled=True)  93 us
    all_gather x1, waiting for transfers between devices, shards(): up_sectioned = lax.all_gather(up_weight, 'sp', axis=0, tiled=True)  83.4 us
    psum x1, waiting for transfers between devices, shards(): lax.psum(jnp.dot(attended, out_weight, preferred_element_type=jnp.float32...  50.9 us
    all_gather x1, waiting for transfers between devices, shards(): gate_sectioned = lax.all_gather(gate_weight, 'sp', axis=0, tiled=True)  38.4 us
    reduce_scatter x1, waiting for transfers between devices, shards(): lax.psum_scatter(jnp.dot(hidden, down_whole, preferred_element_type=jnp.f...  29.5 us
    dot_general x1, matrix products, shards(): jnp.dot(hidden, down_whole, preferred_element_type=jnp.float32)  14.6 us
    dot_general x1, matrix products, shards(): jnp.dot(normed_all, gate_sectioned, preferred_element_type=jnp.float32)  8.96 us
  transfers between devices with their start and end apart: 7, of which 7 were waited for; matrix products, arithmetic and copies ran while one was open for 4% of the time, Pallas kernels for 0%

commit v1 on v0

--- a/solution.py
+++ b/solution.py
@@ -95,8 +95,12 @@
     blocks = lax.map(one_block, jnp.arange(tok_local // block_len, dtype=jnp.int32))
     attended = blocks.reshape(tok_local, queries.shape[1])
     own_first = lax.axis_index("tp") * share_rows
-    attn_full = lax.psum(
-        jnp.dot(attended, out_weight, preferred_element_type=jnp.float32).astype(jnp.bfloat16), "tp"
+    attn_full = jnp.sum(
+        lax.all_gather(
+            jnp.dot(attended, out_weight, preferred_element_type=jnp.float32).astype(jnp.bfloat16),
+            "tp",
+        ),
+        axis=0,
     ).astype(jnp.float32)
     middle_all = residual.astype(jnp.float32) + attn_full
     normed_all = rms_scale(middle_all, norm_gain)

time: 371 us -> 428 us (1.15)
  waiting for transfers between devices: 302 us -> 353 us
  other arithmetic: 10.6 us -> 17.9 us
    all_gather x0 -> x1, waiting for transfers between devices: none -> 57.3 us  [shards(): lax.all_gather(jnp.dot(attended, out_weight, preferred_element_type=jnp.f...]
    psum x1 -> x0, waiting for transfers between devices: 50.9 us -> none  [shards(): lax.psum(jnp.dot(attended, out_weight, preferred_element_type=jnp.float32...]
    all_gather x1, waiting for transfers between devices: 38.4 us -> 82.4 us  [shards(): gate_sectioned = lax.all_gather(gate_weight, 'sp', axis=0, tiled=True)]
    all_gather x1, waiting for transfers between devices: 83.4 us -> 92.6 us  [shards(): up_sectioned = lax.all_gather(up_weight, 'sp', axis=0, tiled=True)]
    all_gather x1, waiting for transfers between devices: 93 us -> 84.5 us  [fetch_down(): return lax.all_gather(down_weight, 'sp', axis=1, tiled=True)]
    reduce_sum x0 -> x1, other arithmetic: none -> 7.22 us  [shards(): jnp.sum(lax.all_gather(jnp.dot(attended, out_weight, preferred_element_ty...]
  transfers between devices with their start and end apart: 7 -> 7, of which waited for: 7 -> 7; matrix products, arithmetic and copies ran while one was open for 4% -> 5% of each run, Pallas kernels for 0% -> 0%
where the time goes in v1:
time: 428 us; the launch traced here: 427 us
  waiting for transfers between devices  353 us (82%)
  matrix products  29.1 us (7%)
  other arithmetic  17.9 us (4%)
  between operations  13.2 us (3%)
  starting transfers between devices  6.5 us (2%)
  local copies, waits for them, and re-layouts  6.13 us (1%)
    all_gather x1, waiting for transfers between devices, shards(): up_sectioned = lax.all_gather(up_weight, 'sp', axis=0, tiled=True)  92.6 us
    all_gather x1, waiting for transfers between devices, fetch_down(): return lax.all_gather(down_weight, 'sp', axis=1, tiled=True)  84.5 us
    all_gather x1, waiting for transfers between devices, shards(): gate_sectioned = lax.all_gather(gate_weight, 'sp', axis=0, tiled=True)  82.4 us
    all_gather x1, waiting for transfers between devices, shards(): lax.all_gather(jnp.dot(attended, out_weight, preferred_element_type=jnp.f...  57.3 us
    reduce_scatter x1, waiting for transfers between devices, shards(): lax.psum_scatter(jnp.dot(hidden, down_whole, preferred_element_type=jnp.f...  29.5 us
    dot_general x1, matrix products, shards(): jnp.dot(hidden, down_whole, preferred_element_type=jnp.float32)  14.5 us
    dot_general x1, matrix products, shards(): jnp.dot(normed_all, gate_sectioned, preferred_element_type=jnp.float32)  8.96 us
  transfers between devices with their start and end apart: 7, of which 7 were waited for; matrix products, arithmetic and copies ran while one was open for 5% of the time, Pallas kernels for 0%

profile of v1, /device:TPU:0, one launch (start us, length us, event | category | flops | bytes accessed | tf_op | source)
XLA Modules:
  0.0 427.3 jit_solution(3487236097310128484)
XLA Ops:
  6.5 1.0 pad_maximum_fusion.2
  7.5 4.9 %collective-permute-start = (bf16[2,128,128]{2,1,0:T(8,128)(2,1)S(1)}, bf16[2,128,128]{2,1,0:T(8,128)(2,1)S(1)}, u32[]{:S(2)}, u32[]{:S(2)}) collective-permute-start(bf16[2,128,128]{2,1,0:T(8,128)(2,1)S(1)} %get-tuple-element.124), channel_id=1, source_target_pairs={{0,4},{4,8},{8,12},{12,16},{16,20},{20,24},{24,28},{1,5},{5,9},{9,... | collective-permute-start | bytes 196616 | tf_op jit(solution)/shard_map/ppermute | solution.py:20
  12.4 1.3 collective-permute-start.1
  13.7 0.6 collective-permute-done
  14.3 4.3 %collective-permute-done.1 = bf16[2,128,128]{2,1,0:T(8,128)(2,1)S(1)} collective-permute-done((bf16[2,128,128]{2,1,0:T(8,128)(2,1)S(1)}, bf16[2,128,128]{2,1,0:T(8,128)(2,1)S(1)}, u32[]{:S(2)}, u32[]{:S(2)}) %collective-permute-start.1) | collective-permute-done | bytes 65568 | tf_op jit(solution)/shard_map/ppermute | solution.py:22
  18.6 1.0 pad_maximum_fusion
  19.6 11.1 %while.12 = (s32[]{:T(128)}, bf16[2,256,512]{2,1,0:T(8,128)(2,1)}, bf16[2,768,128]{2,1,0:T(8,128)(2,1)S(1)}, s32[2]{0:T(128)S(1)}, s32[]{:T(128)}, /*index=5*/bf...) while((s32[]{:T(128)}, bf16[2,256,512]{2,1,0:T(8,128)(2,1)}, ...), condition=%wide.region_3.4_spmd, body=%wide.region_0.3_spmd.sunk | while | flops 273420544 | bytes 14467512 | solution.py:95
  19.6 0.6 dynamic_slice.42
  20.9 0.3 fusion.36
  21.2 1.0 constant_dynamic-slice_fusion.2
  22.1 0.1 copy.26
  22.3 0.5 fusion.37
  22.8 0.1 broadcast_maximum_fusion.2
  22.9 0.3 fusion.38
  23.2 0.1 exponential_add_fusion.2
  23.3 0.5 convolution_convert_fusion.4
  23.8 0.1 copy.27
  24.0 0.4 copy-done.2
  24.4 0.8 copy-done.3
  25.1 0.6 dynamic_slice.42
  26.4 0.3 fusion.36
  26.7 1.0 constant_dynamic-slice_fusion.2
  27.7 0.1 copy.26
  27.9 0.5 fusion.37
  28.4 0.1 broadcast_maximum_fusion.2
  28.4 0.3 fusion.38
  28.7 0.1 exponential_add_fusion.2
  28.8 0.5 convolution_convert_fusion.4
  29.4 0.1 copy.27
  29.5 0.4 copy-done.2
  29.9 0.8 copy-done.3
  30.7 3.6 convolution_convert_fusion.1
  34.4 0.0 all-gather.6.cloned.1.call-start
  34.4 0.7 all-gather.6.cloned.1.call-update
  35.1 0.0 all-gather.10.cloned.1.call-start
  35.2 0.7 all-gather.10.cloned.1.call-update
  35.9 0.5 all-gather.8.cloned.1.call-update
  36.4 0.2 reduce-scatter.2.cloned.1.call-start
  36.6 57.3 %all-gather.12.cloned.1.call-done = bf16[2048,2048]{1,0:T(8,128)(2,1)} async-done(((bf16[512,2048]{1,0:T(8,128)(2,1)}), bf16[2048,2048]{1,0:T(8,128)(2,1)}) %all-gather.12.cloned.1.call-update) | async-done | bytes 8388624 | tf_op jit(solution)/shard_map/all_gather | solution.py:99
  94.0 7.2 %reduce_sum.30 = bf16[512,2048]{1,0:T(8,128)(2,1)} reduce(bf16[4,512,2048]{2,1,0:T(8,128)(2,1)} %bitcast.50, bf16[]{:T(256)} %constant.90.clone.1), dimensions={0}, to_apply=%region_4.5 | reduce | flops 3145728 | bytes 10485762 | tf_op jit(solution)/shard_map/reduce_sum | solution.py:98
  101.2 4.9 %convert_add_fusion = (f32[512,2048]{1,0:T(8,128)}, f32[512]{0:T(512)S(1)}) fusion(bf16[512,2048]{1,0:T(8,128)(2,1)} %reduce_sum.30, bf16[512,2048]{1,0:T(8,128)(2,1)} %param.16), kind=kLoop, calls=%fused_computation.25 | loop fusion | flops 5242368 | bytes 8390656 | tf_op jit(solution)/shard_map/add | solution.py:105
  106.1 82.4 %all-gather.6.cloned.1.call-done = bf16[2048,1408]{1,0:T(8,128)(2,1)} async-done(((bf16[256,1408]{1,0:T(8,128)(2,1)}), bf16[2048,1408]{1,0:T(8,128)(2,1)}) %all-gather.6.cloned.1.call-update) | async-done | bytes 5767184 | tf_op jit(solution)/shard_map/all_gather | solution.py:108
  188.5 9.0 %fusion.14 = f32[512,1408]{1,0:T(8,128)} fusion(bf16[2048,1408]{1,0:T(8,128)(2,1)} %all-gather.6.cloned.1.call-done, f32[2048]{0:T(1024)S(1)} %copy-done.4, f32[512]{0:T(512)S(1)} %add_rsqrt_fusion, bf16[512,2048]{1,0:T(8,128)(2,1)} %reduce_sum.30, bf16[512,2048]{1,0:T(8,128)(2,1)} %param.16), kind=kOutput, calls=%fused_computation.36 | convolution fusion | flops 2959081472 | bytes 12855296 | tf_op jit(solution)/shard_map/dot_general | solution.py:110
  197.5 84.5 %all-gather.10.cloned.1.call-done = bf16[1408,2048]{1,0:T(8,128)(2,1)} async-done(((bf16[1408,256]{1,0:T(8,128)(2,1)}), bf16[1408,2048]{1,0:T(8,128)(2,1)}) %all-gather.10.cloned.1.call-update) | async-done | bytes 5767184 | tf_op jit(solution)/shard_map/all_gather | solution.py:61
  281.9 92.6 %all-gather.8.cloned.1.call-done = bf16[2048,1408]{1,0:T(8,128)(2,1)} async-done(((bf16[256,1408]{1,0:T(8,128)(2,1)}), bf16[2048,1408]{1,0:T(8,128)(2,1)}) %all-gather.8.cloned.1.call-update) | async-done | bytes 5767184 | tf_op jit(solution)/shard_map/all_gather | solution.py:109
  374.5 14.5 %convolution_convert_fusion.2 = bf16[512,2048]{1,0:T(8,128)(2,1)} fusion(bf16[1408,2048]{1,0:T(8,128)(2,1)} %all-gather.10.cloned.1.call-done, bf16[2048,1408]{1,0:T(8,128)(2,1)} %all-gather.8.cloned.1.call-done, f32[512,1408]{1,0:T(8,128)} %fusion.14, f32[2048]{0:T(1024)S(1)} %copy-done.4, f32[512]{0:T(512)S(1)} %add_rsqrt_fusion, ...), kind=kOutput, calls=%fused_computation.29 | convolution fusion | flops 5917245440 | bytes 20719616 | tf_op jit(solution)/shard_map/dot_general | solution.py:115
  389.0 29.5 %reduce-scatter.2.cloned.1.call-done = bf16[128,2048]{1,0:T(8,128)(2,1)} async-done(((bf16[512,2048]{1,0:T(8,128)(2,1)}), bf16[128,2048]{1,0:T(8,128)(2,1)}) %reduce-scatter.2.cloned.1.call-update) | async-done | bytes 524304 | tf_op jit(solution)/shard_map/reduce_scatter | solution.py:114
  418.5 2.3 add_convert_fusion
  (29 shorter events, 0.2 us)
Async XLA Ops:
  6.5 24.2 %copy-start = (bf16[512,2048]{1,0:T(8,128)(2,1)S(1)}, bf16[512,2048]{1,0:T(8,128)(2,1)}, u32[]{:S(2)}) copy-start(bf16[512,2048]{1,0:T(8,128)(2,1)} %param.18) | copy-start | bytes 6291460
  6.5 87.4 %all-gather.12.cloned.1.call-start = ((), (), s32[]{:S(2)}) async-start(), calls=%async_computation.5 | async-start | bytes 10485760 | tf_op jit(solution)/shard_map/all_gather | solution.py:99
  7.5 6.8 %collective-permute-start = (bf16[2,128,128]{2,1,0:T(8,128)(2,1)S(1)}, bf16[2,128,128]{2,1,0:T(8,128)(2,1)S(1)}, u32[]{:S(2)}, u32[]{:S(2)}) collective-permute-start(bf16[2,128,128]{2,1,0:T(8,128)(2,1)S(1)} %get-tuple-element.124), channel_id=1, source_target_pairs={{0,4},{4,8},{8,12},{12,16},{16,20},{20,24},{24,28},{1,5},{5,9},{9,... | collective-permute-start | bytes 196616 | tf_op jit(solution)/shard_map/ppermute | solution.py:20
  12.4 6.2 %collective-permute-start.1 = (bf16[2,128,128]{2,1,0:T(8,128)(2,1)S(1)}, bf16[2,128,128]{2,1,0:T(8,128)(2,1)S(1)}, u32[]{:S(2)}, u32[]{:S(2)}) collective-permute-start(bf16[2,128,128]{2,1,0:T(8,128)(2,1)S(1)} %get-tuple-element.125), channel_id=1, source_target_pairs={{4,0},{8,4},{12,8},{16,12},{20,16},{24,20},{28,24},{5,1},{9,5},{13... | collective-permute-start | bytes 196616 | tf_op jit(solution)/shard_map/ppermute | solution.py:22
  19.6 3.2 copy-start.1
  23.3 1.0 copy-start.2
  24.3 0.8 copy-start.3
  25.1 3.2 copy-start.1
  28.8 1.0 copy-start.2
  29.9 0.8 copy-start.3
  34.4 154.1 %all-gather.6.cloned.1.call-start = ((), (), s32[]{:S(2)}) async-start(), calls=%async_computation.1 | async-start | bytes 6488064 | tf_op jit(solution)/shard_map/all_gather | solution.py:108
  35.1 246.8 %all-gather.10.cloned.1.call-start = ((), (), s32[]{:S(2)}) async-start(), calls=%async_computation.3 | async-start | bytes 6488064 | tf_op jit(solution)/shard_map/all_gather | solution.py:61
  35.8 338.6 %all-gather.8.cloned.1.call-start = ((), (), s32[]{:S(2)}) async-start(), calls=%async_computation.2 | async-start | bytes 6488064 | tf_op jit(solution)/shard_map/all_gather | solution.py:109
  36.4 382.1 %reduce-scatter.2.cloned.1.call-start = ((), (), s32[]{:S(2)}) async-start(), calls=%async_computation.4 | async-start | bytes 2621440 | tf_op jit(solution)/shard_map/reduce_scatter | solution.py:114
  101.2 87.3 %copy-start.4 = (f32[2048]{0:T(1024)S(1)}, f32[2048]{0:T(1024)}, u32[]{:S(2)}) copy-start(f32[2048]{0:T(1024)} %param.17) | copy-start | bytes 24580
Sparse Core Ops, SparseCore 0:
  34.5 59.4 all-gather.11
  96.2 92.2 all-gather.5
  190.5 91.3 all-gather.9
  283.9 90.4 all-gather.7
  389.1 29.3 reduce-scatter.1
